TPU v7x, 32 devices: a whole 2x2x4 slice. The times are simulated.
32 devices in a mesh: gr: 2 (over x), fs: 8 (over z, y), tp: 2 (over core).
Axes of the slice: x: 2, y: 2, z: 4, core: 2. Of those that a mesh axis runs over, the one named last changes fastest.
Arguments:
- tokens: bfloat16 [4096, 2048], P(('gr', 'fs', 'tp')), may hold values from -6 to 6
- norm_gain: float32 [2048], P(('gr', 'fs')), may hold values from 0.1 to 1.9
- up_weight: float32 [2048, 8192], P(('gr', 'fs'), 'tp'), may hold values from -0.125 to 0.125
- down_weight: float32 [8192, 2048], P(('gr', 'fs'), 'tp'), may hold values from -0.0625 to 0.0625
Outputs:
- served: bfloat16 [4096, 2048], P(('gr', 'fs', 'tp'))
- serve_up: bfloat16 [2048, 8192], P(None, 'fs')
- serve_down: bfloat16 [8192, 2048], P('fs')
All inputs are finite; a program needn't handle non-finite values.
Results may differ from a plain program's by a relative error of at most 0.017.
Values may be sent and summed in bfloat16 or wider, within the bound.
A program may use at most 64 MiB of HBM per device.

v0:
```python
import jax
import jax.numpy as jnp
from jax import lax
from jax.sharding import PartitionSpec as P


def body(tokens, norm_gain, up_weight, down_weight):
    groups = lax.axis_size("gr")
    shards = lax.axis_size("fs")
    segment = down_weight.shape[0]
    own_rows = up_weight.shape[0]
    up_local = (norm_gain[:, None] * up_weight).astype(jnp.bfloat16)
    down_local = down_weight.astype(jnp.bfloat16)
    up_cols, down_cols = (
        lax.all_gather(up_local, "tp", axis=1, tiled=True),
        lax.all_gather(down_local, "tp", axis=1, tiled=True),
    )
    width = up_cols.shape[1]
    up_sorted = (
        up_cols.reshape(own_rows, groups, shards, segment)
        .transpose(0, 2, 1, 3)
        .reshape(own_rows, width)
    )
    up_mine = lax.all_to_all(up_sorted, "fs", split_axis=1, concat_axis=0, tiled=True)
    serve_up, serve_down = (
        lax.all_gather(up_mine, "gr", axis=0, tiled=True),
        lax.all_gather(down_cols, "gr", axis=0, tiled=True),
    )
    values = tokens.astype(jnp.float32)
    normed = (values * lax.rsqrt(jnp.mean(values * values, axis=1, keepdims=True) + 1e-06)).astype(
        jnp.bfloat16
    )
    product = jnp.dot(
        lax.all_gather(normed, "fs", axis=0, tiled=True),
        serve_up,
        preferred_element_type=jnp.float32,
    )
    hidden = jnp.square(jax.nn.relu(product)).astype(jnp.bfloat16)
    part = jnp.dot(hidden, serve_down, preferred_element_type=jnp.float32).astype(jnp.bfloat16)
    part = lax.optimization_barrier(part)
    summed = lax.psum_scatter(
        part.astype(jnp.float32).astype(jnp.bfloat16), "fs", scatter_dimension=0, tiled=True
    )
    return (summed, serve_up, serve_down)


def solution(mesh):
    return jax.shard_map(
        body,
        mesh=mesh,
        in_specs=(
            P(("gr", "fs", "tp"), None),
            P(("gr", "fs")),
            P(("gr", "fs"), "tp"),
            P(("gr", "fs"), "tp"),
        ),
        out_specs=(P(("gr", "fs", "tp"), None), P(None, "fs"), P("fs", None)),
        check_vma=False,
    )
```

profile of v0, /device:TPU:0, one launch (start us, length us, event | category | flops | bytes accessed | tf_op | source)
XLA Modules:
  0.0 345.5 jit_solution(10217558467831381124)
XLA Ops:
  7.2 0.0 copy-start.1
  7.2 0.0 copy-start.3
  7.2 0.0 all-gather.12.cloned.1.call-start
  7.2 2.9 convert_element_type.24
  10.1 0.0 copy-start.2
  10.1 0.0 all-gather.12.cloned.1.call-update
  10.1 0.0 all-gather.8.cloned.1.call-start
  10.2 0.0 copy-done.1
  10.2 0.0 copy-done.3
  10.2 1.2 multiply_convert_fusion.1
  11.4 0.0 all-gather.8.cloned.1.call-update
  11.4 0.0 all-gather.14.cloned.1.call-start
  11.4 12.1 %all-gather.12.cloned.1.call-done = bf16[512,2048]{1,0:T(8,128)(2,1)} async-done(((bf16[512,1024]{1,0:T(8,128)(2,1)}), bf16[512,2048]{1,0:T(8,128)(2,1)}) %all-gather.12.cloned.1.call-update) | async-done | bytes 2097168 | tf_op jit(solution)/shard_map/all_gather | solution.py:16
  23.6 0.0 all-gather.14.cloned.1.call-update
  23.6 0.0 all-gather.6.cloned.1.call-start
  23.6 0.0 copy-done.2
  23.7 0.2 fusion
  23.9 1.0 fusion.1
  24.8 0.0 all-gather.6.cloned.1.call-update
  24.8 0.0 all-gather.10.cloned.1.call-start
  24.9 12.6 %all-gather.8.cloned.1.call-done = bf16[128,8192]{1,0:T(8,128)(2,1)} async-done(((bf16[128,4096]{1,0:T(8,128)(2,1)}), bf16[128,8192]{1,0:T(8,128)(2,1)}) %all-gather.8.cloned.1.call-update) | async-done | bytes 2097168 | tf_op jit(solution)/shard_map/all_gather | solution.py:15
  37.5 2.4 copy.8
  39.9 1.6 copy.7
  41.5 2.7 all_to_all.14
  44.2 54.5 %all_to_all.19 = bf16[128,8,1024]{2,0,1:T(8,128)(2,1)} all-to-all(bf16[128,8,1024]{2,0,1:T(8,128)(2,1)} %all_to_all.14), channel_id=1, replica_groups=mesh['gr'=2,'fs'=8,'tp'=2] {'fs'}, dimensions={1} | all-to-all | bytes 4194304 | tf_op jit(solution)/shard_map/all_to_all | solution.py:24
  98.8 0.0 all-gather.10.cloned.1.call-update
  98.8 0.0 reduce-scatter.2.cloned.1.call-start
  98.8 0.0 all-gather.14.cloned.1.call-done
  98.9 73.5 %all-gather.6.cloned.1.call-done = bf16[1024,2048]{1,0:T(8,128)(2,1)} async-done(((bf16[128,2048]{1,0:T(8,128)(2,1)}), bf16[1024,2048]{1,0:T(8,128)(2,1)}) %all-gather.6.cloned.1.call-update) | async-done | bytes 4194320 | tf_op jit(solution)/shard_map/all_gather | solution.py:34
  172.3 56.7 %all-gather.10.cloned.1.call-done = bf16[2048,1024]{1,0:T(8,128)(2,1)} async-done(((bf16[1024,1024]{1,0:T(8,128)(2,1)}), bf16[2048,1024]{1,0:T(8,128)(2,1)}) %all-gather.10.cloned.1.call-update) | async-done | bytes 4194320 | tf_op jit(solution)/shard_map/all_gather | solution.py:26
  229.0 14.4 %convolution_convert_fusion = bf16[1024,2048]{1,0:T(8,128)(2,1)} fusion(bf16[1024,2048]{1,0:T(8,128)(2,1)} %all-gather.14.cloned.1.call-done, bf16[1024,2048]{1,0:T(8,128)(2,1)} %all-gather.6.cloned.1.call-done, bf16[2048,1024]{1,0:T(8,128)(2,1)} %all-gather.10.cloned.1.call-done), kind=kOutput, calls=%fused_computation.1 | convolution fusion | flops 8595177472 | bytes 16777216 | tf_op jit(solution)/shard_map/dot_general | solution.py:39
  243.4 0.0 reduce-scatter.2.cloned.1.call-update
  243.4 88.5 %reduce-scatter.2.cloned.1.call-done = bf16[128,2048]{1,0:T(8,128)(2,1)} async-done(((bf16[1024,2048]{1,0:T(8,128)(2,1)}), bf16[128,2048]{1,0:T(8,128)(2,1)}) %reduce-scatter.2.cloned.1.call-update) | async-done | bytes 524304 | tf_op jit(solution)/shard_map/reduce_scatter | solution.py:41
  331.9 0.0 copy-start
  331.9 4.8 %copy.11 = bf16[2048,1024]{1,0:T(8,128)(2,1)} copy(bf16[2048,1024]{1,0:T(8,128)(2,1)} %all-gather.10.cloned.1.call-done) | data formatting | bytes 8388608
  336.7 0.0 copy-done
  336.7 2.0 copy.12
  (1 shorter events, 0.0 us)
Async XLA Ops:
  7.2 3.0 copy-start.1
  7.2 3.0 copy-start.3
  7.2 16.4 %all-gather.12.cloned.1.call-start = ((), (), s32[]{:S(2)}) async-start(), calls=%async_computation.5 | async-start | bytes 3145728 | tf_op jit(solution)/shard_map/all_gather | solution.py:16
  10.1 13.6 %copy-start.2 = (bf16[128,2048]{1,0:T(8,128)(2,1)S(1)}, bf16[128,2048]{1,0:T(8,128)(2,1)}, u32[]{:S(2)}) copy-start(bf16[128,2048]{1,0:T(8,128)(2,1)} %param.4) | copy-start | bytes 1572868
  10.1 27.4 %all-gather.8.cloned.1.call-start = ((), (), s32[]{:S(2)}) async-start(), calls=%async_computation.3 | async-start | bytes 3145728 | tf_op jit(solution)/shard_map/all_gather | solution.py:15
  11.4 87.5 %all-gather.14.cloned.1.call-start = ((), (), s32[]{:S(2)}) async-start(), calls=%async_computation.6 | async-start | bytes 6291456 | tf_op jit(solution)/shard_map/all_gather | solution.py:27
  23.6 148.7 %all-gather.6.cloned.1.call-start = ((), (), s32[]{:S(2)}) async-start(), calls=%async_computation.2 | async-start | bytes 4718592 | tf_op jit(solution)/shard_map/all_gather | solution.py:34
  24.8 204.2 %all-gather.10.cloned.1.call-start = ((), (), s32[]{:S(2)}) async-start(), calls=%async_computation.4 | async-start | bytes 6291456 | tf_op jit(solution)/shard_map/all_gather | solution.py:26
  98.8 233.1 %reduce-scatter.2.cloned.1.call-start = ((), (), s32[]{:S(2)}) async-start(), calls=%async_computation.7 | async-start | bytes 4718592 | tf_op jit(solution)/shard_map/reduce_scatter | solution.py:41
  331.9 4.8 %copy-start = (bf16[1024,2048]{1,0:T(8,128)(2,1)S(1)}, bf16[1024,2048]{1,0:T(8,128)(2,1)}, u32[]{:S(2)}) copy-start(bf16[1024,2048]{1,0:T(8,128)(2,1)} %all-gather.14.cloned.1.call-done) | copy-start | bytes 12582916
Sparse Core Ops, SparseCore 0:
  10.2 13.2 all-gather.11
  25.7 11.7 all-gather.7
  39.0 57.8 all-gather.13
  99.5 72.7 all-gather.5
  173.7 55.2 all-gather.9
  243.5 88.2 reduce-scatter.1
where the time goes:
time: 346 us
  waiting for transfers between devices  243 us (70%)
  blocking collectives  54.5 us (16%)
  matrix products  14.4 us (4%)
  between operations  14.2 us (4%)
  local copies, waits for them, and re-layouts  13.6 us (4%)
  other arithmetic  5.2 us (2%)
    reduce_scatter x1, waiting for transfers between devices, body(): lax.psum_scatter(part.astype(jnp.float32).astype(jnp.bfloat16), 'fs', sca...  88.5 us
    all_gather x1, waiting for transfers between devices, body(): lax.all_gather(normed, 'fs', axis=0, tiled=True)  73.5 us
    all_gather x1, waiting for transfers between devices, body(): lax.all_gather(up_mine, 'gr', axis=0, tiled=True)  56.7 us
    all_to_all x1, blocking collectives, body(): lax.all_to_all(up_sorted, 'fs', split_axis=1, concat_axis=0, tiled=True)  54.5 us
    dot_general x1, matrix products, body(): jnp.dot(hidden, serve_down, preferred_element_type=jnp.float32)  14.4 us
    all_gather x1, waiting for transfers between devices, body(): lax.all_gather(up_local, 'tp', axis=1, tiled=True)  12.6 us
    all_gather x1, waiting for transfers between devices, body(): lax.all_gather(down_local, 'tp', axis=1, tiled=True)  12.1 us
    unnamed x11, local copies, waits for them, and re-layouts  9.26 us
  transfers between devices with their start and end apart: 6, of which 5 were waited for; matrix products, arithmetic and copies ran while one was open for 2% of the time, Pallas kernels for 0%

commit v1 on v0

v1 whole, which is shorter than its diff:
```python
import functools

import jax
import jax.numpy as jnp
from jax import lax
from jax.experimental import pallas as pl
from jax.experimental.pallas import tpu as pltpu
from jax.sharding import PartitionSpec as P

MESH = pl.DeviceIdType.MESH
TILE = 256


def kernel(sizes, normed, up, down, served, out_up, out_down, tok, su, sd, hid, part, got, *sems):
    groups, shards, cores = sizes
    (up_send, up_recv, gu_send, gu_recv, tu_send, tu_recv, gd_send, gd_recv,
     td_send, td_recv, tok_send, tok_recv, part_send, part_recv, local, out_sem) = sems
    g, f, t = lax.axis_index("gr"), lax.axis_index("fs"), lax.axis_index("tp")
    rows, depth = normed.shape
    own_rows = up.shape[0]
    segment, dcols = down.shape
    nseg = up.shape[1] // segment
    group_rows = shards * own_rows

    def to(axis, me, size, step):
        return {axis: lax.rem(me + step, size)}

    def rdma(src, dst, send, recv, device):
        return pltpu.make_async_remote_copy(
            src_ref=src, dst_ref=dst, send_sem=send, recv_sem=recv,
            device_id=device, device_id_type=MESH,
        )

    peers = [to("fs", f, shards, k) for k in range(1, shards)]
    peers += [to("gr", g, groups, k) for k in range(1, groups)]
    peers += [to("tp", t, cores, k) for k in range(1, cores)]
    barrier = pltpu.get_barrier_semaphore()
    for peer in peers:
        pl.semaphore_signal(barrier, inc=1, device_id=peer, device_id_type=MESH)
    pl.semaphore_wait(barrier, len(peers))

    def up_block(group, shard, sg):
        row = pl.multiple_of((group * shards + shard) * own_rows, own_rows)
        return su.at[pl.ds(row, own_rows), pl.ds(pl.multiple_of(sg * segment, segment), segment)]

    def up_group(group, sg):
        row = pl.multiple_of(group * group_rows, group_rows)
        return su.at[pl.ds(row, group_rows), pl.ds(sg * segment, segment)]

    def down_block(group, core):
        row = pl.multiple_of(group * segment, segment)
        return sd.at[pl.ds(row, segment), pl.ds(pl.multiple_of(core * dcols, dcols), dcols)]

    def owner(sg):
        return (sg * shards + f) // nseg

    def up_copy(i):
        number = t * nseg + i
        shard, sg = lax.rem(number, shards), number // shards
        step = lax.rem(shard - f + shards, shards)
        src = up.at[:, pl.ds(pl.multiple_of(i * segment, segment), segment)]
        remote = rdma(src, up_block(g, f, sg), up_send.at[i], up_recv.at[sg, step], {"fs": shard})
        here = pltpu.make_async_copy(src, up_block(g, f, sg), up_recv.at[sg, 0])
        return shard == f, here, remote

    def start_up(j, carry):
        mine, here, remote = up_copy(lax.rem(f + j, nseg))
        pl.when(mine)(here.start)
        pl.when(jnp.logical_not(mine))(remote.start)
        return carry

    lax.fori_loop(0, nseg, start_up, 0)

    sends = []
    keep_down = pltpu.make_async_copy(down, down_block(g, t), local.at[0])
    keep_tok = pltpu.make_async_copy(normed, tok.at[pl.ds((shards - 1) * rows, rows)], local.at[1])
    keep_down.start()
    keep_tok.start()
    down_in = []
    for k in range(1, groups):
        copy = rdma(down, down_block(g, t), gd_send.at[k], gd_recv.at[k], to("gr", g, groups, k))
        copy.start()
        sends.append(copy)
        source = lax.rem(g + groups - k, groups)
        down_in.append((k, source))
    for k in range(1, cores):
        copy = rdma(down, down_block(g, t), td_send.at[k, 0], td_recv.at[k, 0], to("tp", t, cores, k))
        copy.start()
        sends.append(copy)

    for k in range(1, shards):
        copy = rdma(normed, tok.at[pl.ds((k - 1) * rows, rows)], tok_send.at[k], tok_recv.at[k],
                    to("fs", f, shards, k))
        copy.start()
        sends.append(copy)

    for sg in range(groups):
        def forward(sg=sg):
            def arrived(k, carry):
                shard = lax.rem(f + shards - k, shards)
                block = up_block(g, shard, sg)
                if True:
                    @pl.when(k == 0)
                    def _():
                        pltpu.make_async_copy(block, block, up_recv.at[sg, 0]).wait()

                    @pl.when(k > 0)
                    def _():
                        rdma(block, block, up_send.at[0], up_recv.at[sg, k], {"fs": shard}).wait_recv()
                for d in range(1, groups):
                    rdma(block, block, gu_send.at[sg, d, k], gu_recv.at[sg, d, k],
                         to("gr", g, groups, d)).start()
                return carry

            lax.fori_loop(0, shards, arrived, 0)
            whole = up_group(g, sg)
            for c in range(1, cores):
                rdma(whole, whole, tu_send.at[sg, 0, c], tu_recv.at[sg, 0], to("tp", t, cores, c)).start()

        pl.when(owner(sg) == t)(forward)

    for k, source in down_in:
        block = down_block(source, t)
        rdma(block, block, gd_send.at[k], gd_recv.at[k], {"gr": source}).wait_recv()
        for c in range(1, cores):
            copy = rdma(block, block, td_send.at[c, k], td_recv.at[c, k], to("tp", t, cores, c))
            copy.start()
            sends.append(copy)

    for sg in range(groups):
        def onward(sg=sg):
            for d in range(1, groups):
                source = lax.rem(g + groups - d, groups)

                def arrived(k, carry):
                    block = up_block(source, lax.rem(f + shards - k, shards), sg)
                    rdma(block, block, gu_send.at[sg, d, k], gu_recv.at[sg, d, k], {"gr": source}).wait()
                    return carry

                lax.fori_loop(0, shards, arrived, 0)
                whole = up_group(source, sg)
                for c in range(1, cores):
                    rdma(whole, whole, tu_send.at[sg, d, c], tu_recv.at[sg, d],
                         to("tp", t, cores, c)).start()

        pl.when(owner(sg) == t)(onward)

    keep_down.wait()
    keep_tok.wait()
    for c in range(1, cores):
        core = lax.rem(t + cores - c, cores)
        for k in range(groups):
            block = down_block(lax.rem(g + groups - k, groups), core)
            rdma(block, block, td_send.at[c, k], td_recv.at[c, k], {"tp": core}).wait_recv()
    for sg in range(groups):
        def take(sg=sg):
            for d in range(groups):
                whole = up_group(lax.rem(g + groups - d, groups), sg)
                rdma(whole, whole, tu_send.at[sg, d, 1], tu_recv.at[sg, d],
                     {"tp": owner(sg)}).wait_recv()

        pl.when(owner(sg) != t)(take)

    put_up = pltpu.make_async_copy(su, out_up, out_sem.at[0])
    put_down = pltpu.make_async_copy(sd, out_down, out_sem.at[1])
    put_up.start()
    put_down.start()

    def part_copy(k):
        at = pl.ds(pl.multiple_of((k - 1) * rows, rows), rows)
        return rdma(part.at[at], got.at[at], part_send.at[k], part_recv.at[k],
                    {"fs": lax.rem(f + shards - k, shards)})

    width = su.shape[1]

    def pair(j, carry):
        for k in (2 * j + 1, 2 * j + 2):
            at = pl.ds(pl.multiple_of((k - 1) * rows, rows), rows)

            @pl.when(k < shards)
            def _():
                rdma(normed, tok.at[at], tok_send.at[k], tok_recv.at[k],
                     {"fs": lax.rem(f + shards - k, shards)}).wait_recv()

        both = pl.ds(pl.multiple_of(2 * j * rows, 2 * rows), 2 * rows)

        def first(n, carry):
            cols = pl.ds(pl.multiple_of(n * TILE, TILE), TILE)
            product = jnp.dot(tok[both, :], su[:, cols], preferred_element_type=jnp.float32)
            product = jnp.maximum(product, 0.0)
            hid[:, cols] = (product * product).astype(jnp.bfloat16)
            return carry

        lax.fori_loop(0, width // TILE, first, 0)

        def second(n, carry):
            cols = pl.ds(pl.multiple_of(n * TILE, TILE), TILE)
            product = jnp.dot(hid[...], sd[:, cols], preferred_element_type=jnp.float32)
            part[both, cols] = product.astype(jnp.bfloat16)
            return carry

        lax.fori_loop(0, depth // TILE, second, 0)
        for k in (2 * j + 1, 2 * j + 2):
            @pl.when(k < shards)
            def _():
                part_copy(k).start()
        return carry

    lax.fori_loop(0, shards // 2, pair, 0)

    def finish(k, carry):
        part_copy(k).wait()
        return carry

    lax.fori_loop(1, shards, finish, 0)

    def total(r, carry):
        at = pl.multiple_of(r * 16, 16)
        value = part[pl.ds((shards - 1) * rows + at, 16), :].astype(jnp.float32)
        for k in range(1, shards):
            value += got[pl.ds((k - 1) * rows + at, 16), :].astype(jnp.float32)
        served[pl.ds(at, 16), :] = value.astype(jnp.bfloat16)
        return carry

    lax.fori_loop(0, rows // 16, total, 0)

    for copy in sends:
        copy.wait_send()

    def end_up(j, carry):
        mine, here, remote = up_copy(j)
        pl.when(jnp.logical_not(mine))(remote.wait_send)
        return carry

    lax.fori_loop(0, nseg, end_up, 0)
    for sg in range(groups):
        def end(sg=sg):
            for d in range(groups):
                whole = up_group(lax.rem(g + groups - d, groups), sg)
                for c in range(1, cores):
                    rdma(whole, whole, tu_send.at[sg, d, c], tu_recv.at[sg, d],
                         to("tp", t, cores, c)).wait_send()

        pl.when(owner(sg) == t)(end)
    put_up.wait()
    put_down.wait()


def body(tokens, norm_gain, up_weight, down_weight):
    groups, shards, cores = (lax.axis_size(a) for a in ("gr", "fs", "tp"))
    segment = down_weight.shape[0]
    up = (norm_gain[:, None] * up_weight).astype(jnp.bfloat16)
    down = down_weight.astype(jnp.bfloat16)
    values = tokens.astype(jnp.float32)
    normed = (values * lax.rsqrt(jnp.mean(values * values, axis=1, keepdims=True) + 1e-06)).astype(
        jnp.bfloat16
    )
    rows, depth = tokens.shape
    nseg = up.shape[1] // segment
    width = groups * segment
    bf = jnp.bfloat16
    dma = pltpu.SemaphoreType.DMA
    vmem = pl.BlockSpec(memory_space=pltpu.VMEM)
    hbm = pl.BlockSpec(memory_space=pl.ANY)
    return pl.pallas_call(
        functools.partial(kernel, (groups, shards, cores)),
        out_shape=(
            jax.ShapeDtypeStruct((rows, depth), bf),
            jax.ShapeDtypeStruct((depth, width), bf),
            jax.ShapeDtypeStruct((width, depth), bf),
        ),
        in_specs=[vmem] * 3,
        out_specs=(vmem, hbm, hbm),
        scratch_shapes=[
            pltpu.VMEM((shards * rows, depth), bf),
            pltpu.VMEM((depth, width), bf),
            pltpu.VMEM((width, depth), bf),
            pltpu.VMEM((2 * rows, width), bf),
            pltpu.VMEM((shards * rows, depth), bf),
            pltpu.VMEM((shards * rows, depth), bf),
            dma((nseg,)), dma((groups, shards)),
            dma((groups, groups, shards)), dma((groups, groups, shards)),
            dma((groups, groups, cores)), dma((groups, groups)),
            dma((groups,)), dma((groups,)),
            dma((cores, groups)), dma((cores, groups)),
            dma((shards,)), dma((shards,)),
            dma((shards,)), dma((shards,)),
            dma((2,)), dma((2,)),
        ],
        compiler_params=pltpu.CompilerParams(
            collective_id=0, has_side_effects=True, vmem_limit_bytes=48 * 1024 * 1024
        ),
        name="serve",
    )(normed, up, down)


def solution(mesh):
    return jax.shard_map(
        body,
        mesh=mesh,
        in_specs=(
            P(("gr", "fs", "tp"), None),
            P(("gr", "fs")),
            P(("gr", "fs"), "tp"),
            P(("gr", "fs"), "tp"),
        ),
        out_specs=(P(("gr", "fs", "tp"), None), P(None, "fs"), P("fs", None)),
        check_vma=False,
    )
```

time: 346 us -> 254 us (0.73)
  waiting for transfers between devices: 243 us -> 0 us
  Pallas kernels: 0 us -> 240 us
  blocking collectives: 54.5 us -> 0 us
  matrix products: 14.4 us -> 0 us
  between operations: 14.2 us -> 0.67 us
  local copies, waits for them, and re-layouts: 13.6 us -> 7.63 us
    pallas_call x0 -> x1, Pallas kernels: none -> 240 us  [body(): pl.pallas_call(functools.partial(kernel, (groups, shards, cores)), out_sh...]
    all_gather x5 -> x0, waiting for transfers between devices: 155 us -> none  [the longest x1 73.5 us: body(): lax.all_gather(normed, 'fs', axis=0, tiled=True)]
    reduce_scatter x1 -> x0, waiting for transfers between devices: 88.5 us -> none  [body(): lax.psum_scatter(part.astype(jnp.float32).astype(jnp.bfloat16), 'fs', sca...]
    all_to_all x1 -> x0, blocking collectives: 54.5 us -> none  [body(): lax.all_to_all(up_sorted, 'fs', split_axis=1, concat_axis=0, tiled=True)]
    dot_general x1 -> x0, matrix products: 14.4 us -> none  [body(): jnp.dot(hidden, serve_down, preferred_element_type=jnp.float32)]
    unnamed x11 -> x7, local copies, waits for them, and re-layouts: 9.26 us -> 7.63 us
  transfers between devices with their start and end apart: 6 -> 0, of which waited for: 5 -> 0; matrix products, arithmetic and copies ran while one was open for 2% -> 0% of each run, Pallas kernels for 0% -> 0%
where the time goes in v1:
time: 254 us; the launch traced here: 253 us
  Pallas kernels  240 us (94%)
  local copies, waits for them, and re-layouts  7.63 us (3%)
  other arithmetic  4.54 us (2%)
    pallas_call x1, Pallas kernels, body(): pl.pallas_call(functools.partial(kernel, (groups, shards, cores)), out_sh...  240 us
    unnamed x7, local copies, waits for them, and re-layouts  7.63 us

profile of v1, /device:TPU:0, one launch (start us, length us, event | category | flops | bytes accessed | tf_op | source)
XLA Modules:
  0.0 253.3 jit_solution(4845703304586220682)
XLA Ops:
  0.6 1.2 fusion
  1.9 0.0 copy-start.1
  1.9 1.3 fusion.1.normed
  3.2 1.8 multiply_convert_fusion.up
  5.0 0.0 copy-done.1
  5.1 0.2 convert_element_type.15.down
  5.2 240.5 %serve.1 = (bf16[128,2048]{1,0:T(8,128)(2,1)S(1)}, bf16[2048,1024]{1,0:T(8,128)(2,1)}, bf16[1024,2048]{1,0:T(8,128)(2,1)}) custom-call(bf16[128,2048]{1,0:T(8,128)(2,1)S(1)} %fusion.1.normed, bf16[128,4096]{1,0:T(8,128)(2,1)S(1)} %multiply_convert_fusion.up, bf16[512,1024]{1,0:T(8,128)(2,1)S(1)} %convert_element_type.15.down), custom_call_target="tpu_custom_call" | custom-call | tf_op jit(solution)/shard_map/serve/pallas_call | solution.py:265
  245.7 0.8 copy.10
  246.5 0.0 copy-start
  246.5 4.8 %copy.11 = bf16[2048,1024]{1,0:T(8,128)(2,1)} copy(bf16[2048,1024]{1,0:T(8,128)(2,1)} %get-tuple-element.7) | data formatting | bytes 8388608
  251.3 0.0 copy-done
  251.3 2.0 copy.12
  (1 shorter events, 0.0 us)
Async XLA Ops:
  1.9 3.2 %copy-start.1 = (f32[512,1024]{1,0:T(8,128)S(1)}, f32[512,1024]{1,0:T(8,128)}, u32[]{:S(2)}) copy-start(f32[512,1024]{1,0:T(8,128)} %param.7) | copy-start | bytes 6291460
  246.5 4.8 %copy-start = (bf16[1024,2048]{1,0:T(8,128)(2,1)S(1)}, bf16[1024,2048]{1,0:T(8,128)(2,1)}, u32[]{:S(2)}) copy-start(bf16[1024,2048]{1,0:T(8,128)(2,1)} %get-tuple-element.8) | copy-start | bytes 12582916

commit v2 on v1

--- a/solution.py
+++ b/solution.py
@@ -11,11 +11,18 @@
 TILE = 256
 
 
-def kernel(sizes, normed, up, down, served, out_up, out_down, tok, su, sd, hid, part, got, *sems):
+def inner_size(shards):
+    return max(d for d in range(1, shards + 1) if shards % d == 0 and d * d <= shards)
+
+
+def kernel(sizes, normed, up, down, served, out_up, out_down, tok, su, sd, hid, part, got, far, *sems):
     groups, shards, cores = sizes
+    inner = inner_size(shards)
+    outer = shards // inner
     (up_send, up_recv, gu_send, gu_recv, tu_send, tu_recv, gd_send, gd_recv,
-     td_send, td_recv, tok_send, tok_recv, part_send, part_recv, local, out_sem) = sems
+     td_send, td_recv, tok_send, tok_recv, part_send, part_recv, far_send, far_recv, local, out_sem) = sems
     g, f, t = lax.axis_index("gr"), lax.axis_index("fs"), lax.axis_index("tp")
+    z, y = f // inner, lax.rem(f, inner)
     rows, depth = normed.shape
     own_rows = up.shape[0]
     segment, dcols = down.shape
@@ -30,6 +37,15 @@
             src_ref=src, dst_ref=dst, send_sem=send, recv_sem=recv,
             device_id=device, device_id_type=MESH,
         )
+
+    def back(o, i):
+        return {"fs": lax.rem(z + outer - o, outer) * inner + lax.rem(y + inner - i, inner)}
+
+    def ahead(o, i):
+        return {"fs": lax.rem(z + o, outer) * inner + lax.rem(y + i, inner)}
+
+    def block_of(ref, number, count=1):
+        return ref.at[pl.ds(pl.multiple_of(number * rows, rows), count * rows)]
 
     peers = [to("fs", f, shards, k) for k in range(1, shards)]
     peers += [to("gr", g, groups, k) for k in range(1, groups)]
@@ -73,7 +89,7 @@
 
     sends = []
     keep_down = pltpu.make_async_copy(down, down_block(g, t), local.at[0])
-    keep_tok = pltpu.make_async_copy(normed, tok.at[pl.ds((shards - 1) * rows, rows)], local.at[1])
+    keep_tok = pltpu.make_async_copy(normed, block_of(tok, 0), local.at[1])
     keep_down.start()
     keep_tok.start()
     down_in = []
@@ -88,9 +104,9 @@
         copy.start()
         sends.append(copy)
 
-    for k in range(1, shards):
-        copy = rdma(normed, tok.at[pl.ds((k - 1) * rows, rows)], tok_send.at[k], tok_recv.at[k],
-                    to("fs", f, shards, k))
+    for o, i in [(o, 0) for o in range(1, outer)] + [(0, i) for i in range(1, inner)]:
+        n = o * inner + i
+        copy = rdma(normed, block_of(tok, n), tok_send.at[n], tok_recv.at[n], ahead(o, i))
         copy.start()
         sends.append(copy)
 
@@ -99,14 +115,15 @@
             def arrived(k, carry):
                 shard = lax.rem(f + shards - k, shards)
                 block = up_block(g, shard, sg)
-                if True:
-                    @pl.when(k == 0)
-                    def _():
-                        pltpu.make_async_copy(block, block, up_recv.at[sg, 0]).wait()
-
-                    @pl.when(k > 0)
-                    def _():
-                        rdma(block, block, up_send.at[0], up_recv.at[sg, k], {"fs": shard}).wait_recv()
+
+                @pl.when(k == 0)
+                def _():
+                    pltpu.make_async_copy(block, block, up_recv.at[sg, 0]).wait()
+
+                @pl.when(k > 0)
+                def _():
+                    rdma(block, block, up_send.at[0], up_recv.at[sg, k], {"fs": shard}).wait_recv()
+
                 for d in range(1, groups):
                     rdma(block, block, gu_send.at[sg, d, k], gu_recv.at[sg, d, k],
                          to("gr", g, groups, d)).start()
@@ -118,6 +135,15 @@
                 rdma(whole, whole, tu_send.at[sg, 0, c], tu_recv.at[sg, 0], to("tp", t, cores, c)).start()
 
         pl.when(owner(sg) == t)(forward)
+
+    for o in range(1, outer):
+        block = block_of(tok, o * inner)
+        rdma(block, block, tok_send.at[o * inner], tok_recv.at[o * inner], back(o, 0)).wait_recv()
+        for i in range(1, inner):
+            n = o * inner + i
+            copy = rdma(block, block_of(tok, n), tok_send.at[n], tok_recv.at[n], ahead(0, i))
+            copy.start()
+            sends.append(copy)
 
     for k, source in down_in:
         block = down_block(source, t)
@@ -166,23 +192,22 @@
     put_up.start()
     put_down.start()
 
-    def part_copy(k):
-        at = pl.ds(pl.multiple_of((k - 1) * rows, rows), rows)
-        return rdma(part.at[at], got.at[at], part_send.at[k], part_recv.at[k],
-                    {"fs": lax.rem(f + shards - k, shards)})
-
     width = su.shape[1]
-
-    def pair(j, carry):
-        for k in (2 * j + 1, 2 * j + 2):
-            at = pl.ds(pl.multiple_of((k - 1) * rows, rows), rows)
-
-            @pl.when(k < shards)
-            def _():
-                rdma(normed, tok.at[at], tok_send.at[k], tok_recv.at[k],
-                     {"fs": lax.rem(f + shards - k, shards)}).wait_recv()
-
-        both = pl.ds(pl.multiple_of(2 * j * rows, 2 * rows), 2 * rows)
+    stack = inner * rows
+
+    def near_copy(o, i):
+        n = o * inner + i
+        return rdma(block_of(part, n), block_of(got, n), part_send.at[n], part_recv.at[n], back(0, i))
+
+    def far_copy(o):
+        return rdma(block_of(part, o * inner), block_of(far, o), far_send.at[o], far_recv.at[o], back(o, 0))
+
+    def compute(o):
+        for i in range(1, inner):
+            block = block_of(tok, o * inner + i)
+            n = o * inner + i
+            rdma(block, block, tok_send.at[n], tok_recv.at[n], back(0, i)).wait_recv()
+        both = pl.ds(pl.multiple_of(o * stack, stack), stack)
 
         def first(n, carry):
             cols = pl.ds(pl.multiple_of(n * TILE, TILE), TILE)
@@ -200,25 +225,49 @@
             return carry
 
         lax.fori_loop(0, depth // TILE, second, 0)
-        for k in (2 * j + 1, 2 * j + 2):
-            @pl.when(k < shards)
-            def _():
-                part_copy(k).start()
-        return carry
-
-    lax.fori_loop(0, shards // 2, pair, 0)
-
-    def finish(k, carry):
-        part_copy(k).wait()
-        return carry
-
-    lax.fori_loop(1, shards, finish, 0)
+        for i in range(1, inner):
+            near_copy(o, i).start()
+
+    def gather(o):
+        for i in range(1, inner):
+            near_copy(o, i).wait()
+
+    def add(o):
+        gather(o)
+
+        def chunk(r, carry):
+            at = pl.multiple_of(r * 16, 16)
+            mine = pl.ds(pl.multiple_of(o * stack + at, 16), 16)
+            value = part[mine, :].astype(jnp.float32)
+            for i in range(1, inner):
+                value += got[pl.ds(pl.multiple_of(o * stack + i * rows + at, 16), 16), :].astype(jnp.float32)
+            part[mine, :] = value.astype(jnp.bfloat16)
+            return carry
+
+        lax.fori_loop(0, rows // 16, chunk, 0)
+        far_copy(o).start()
+
+    def step(o, carry):
+        compute(lax.rem(o, outer))
+        pl.when(o > 1)(lambda: add(o - 1))
+        return carry
+
+    lax.fori_loop(1, outer + 1, step, 0)
+    gather(0)
+
+    def finish(o, carry):
+        far_copy(o).wait()
+        return carry
+
+    lax.fori_loop(1, outer, finish, 0)
 
     def total(r, carry):
         at = pl.multiple_of(r * 16, 16)
-        value = part[pl.ds((shards - 1) * rows + at, 16), :].astype(jnp.float32)
-        for k in range(1, shards):
-            value += got[pl.ds((k - 1) * rows + at, 16), :].astype(jnp.float32)
+        value = part[pl.ds(at, 16), :].astype(jnp.float32)
+        for i in range(1, inner):
+            value += got[pl.ds(pl.multiple_of(i * rows + at, 16), 16), :].astype(jnp.float32)
+        for o in range(1, outer):
+            value += far[pl.ds(pl.multiple_of(o * rows + at, 16), 16), :].astype(jnp.float32)
         served[pl.ds(at, 16), :] = value.astype(jnp.bfloat16)
         return carry
 
@@ -256,6 +305,7 @@
         jnp.bfloat16
     )
     rows, depth = tokens.shape
+    inner = inner_size(shards)
     nseg = up.shape[1] // segment
     width = groups * segment
     bf = jnp.bfloat16
@@ -275,9 +325,10 @@
             pltpu.VMEM((shards * rows, depth), bf),
             pltpu.VMEM((depth, width), bf),
             pltpu.VMEM((width, depth), bf),
-            pltpu.VMEM((2 * rows, width), bf),
+            pltpu.VMEM((inner * rows, width), bf),
             pltpu.VMEM((shards * rows, depth), bf),
             pltpu.VMEM((shards * rows, depth), bf),
+            pltpu.VMEM((shards // inner * rows, depth), bf),
             dma((nseg,)), dma((groups, shards)),
             dma((groups, groups, shards)), dma((groups, groups, shards)),
             dma((groups, groups, cores)), dma((groups, groups)),
@@ -285,6 +336,7 @@
             dma((cores, groups)), dma((cores, groups)),
             dma((shards,)), dma((shards,)),
             dma((shards,)), dma((shards,)),
+            dma((shards // inner,)), dma((shards // inner,)),
             dma((2,)), dma((2,)),
         ],
         compiler_params=pltpu.CompilerParams(

time: 254 us -> 169 us (0.67)
  Pallas kernels: 240 us -> 156 us
    pallas_call x1, Pallas kernels: 240 us -> 156 us  [body(): pl.pallas_call(functools.partial(kernel, (groups, shards, cores)), out_sh...]
where the time goes in v2:
time: 169 us
  Pallas kernels  156 us (92%)
  local copies, waits for them, and re-layouts  7.63 us (5%)
  other arithmetic  4.54 us (3%)
    pallas_call x1, Pallas kernels, body(): pl.pallas_call(functools.partial(kernel, (groups, shards, cores)), out_sh...  156 us
    unnamed x7, local copies, waits for them, and re-layouts  7.63 us

profile of v2, /device:TPU:0, one launch (start us, length us, event | category | flops | bytes accessed | tf_op | source)
XLA Modules:
  0.0 168.7 jit_solution(17579198779448484598)
XLA Ops:
  0.6 1.2 fusion
  1.9 0.0 copy-start.1
  1.9 1.3 fusion.1.normed
  3.2 1.8 %multiply_convert_fusion.up = bf16[128,4096]{1,0:T(8,128)(2,1)S(1)} fusion(f32[128,4096]{1,0:T(8,128)} %param.6, f32[128]{0:T(128)} %param.5), kind=kLoop, calls=%fused_computation | loop fusion | flops 1048576 | bytes 3146240 | tf_op jit(solution)/shard_map/convert_element_type | solution.py:301
  5.0 0.0 copy-done.1
  5.1 0.2 convert_element_type.15.down
  5.2 155.9 %serve.1 = (bf16[128,2048]{1,0:T(8,128)(2,1)S(1)}, bf16[2048,1024]{1,0:T(8,128)(2,1)}, bf16[1024,2048]{1,0:T(8,128)(2,1)}) custom-call(bf16[128,2048]{1,0:T(8,128)(2,1)S(1)} %fusion.1.normed, bf16[128,4096]{1,0:T(8,128)(2,1)S(1)} %multiply_convert_fusion.up, bf16[512,1024]{1,0:T(8,128)(2,1)S(1)} %convert_element_type.15.down), custom_call_target="tpu_custom_call" | custom-call | tf_op jit(solution)/shard_map/serve/pallas_call | solution.py:315
  161.1 0.8 copy.10
  161.9 0.0 copy-start
  161.9 4.8 %copy.11 = bf16[2048,1024]{1,0:T(8,128)(2,1)} copy(bf16[2048,1024]{1,0:T(8,128)(2,1)} %get-tuple-element.7) | data formatting | bytes 8388608
  166.7 0.0 copy-done
  166.7 2.0 %copy.12 = bf16[1024,2048]{1,0:T(8,128)(2,1)} copy(bf16[1024,2048]{1,0:T(8,128)(2,1)S(1)} %copy-done) | data formatting | bytes 8388608
  (1 shorter events, 0.0 us)
Async XLA Ops:
  1.9 3.2 %copy-start.1 = (f32[512,1024]{1,0:T(8,128)S(1)}, f32[512,1024]{1,0:T(8,128)}, u32[]{:S(2)}) copy-start(f32[512,1024]{1,0:T(8,128)} %param.7) | copy-start | bytes 6291460
  161.9 4.8 %copy-start = (bf16[1024,2048]{1,0:T(8,128)(2,1)S(1)}, bf16[1024,2048]{1,0:T(8,128)(2,1)}, u32[]{:S(2)}) copy-start(bf16[1024,2048]{1,0:T(8,128)(2,1)} %get-tuple-element.8) | copy-start | bytes 12582916

commit v3 on v2

--- a/solution.py
+++ b/solution.py
@@ -20,7 +20,7 @@
     inner = inner_size(shards)
     outer = shards // inner
     (up_send, up_recv, gu_send, gu_recv, tu_send, tu_recv, gd_send, gd_recv,
-     td_send, td_recv, tok_send, tok_recv, part_send, part_recv, far_send, far_recv, local, out_sem) = sems
+     td_send, td_recv, tok_send, tok_recv, part_send, part_recv, far_send, far_recv, hop_send, local, out_sem) = sems
     g, f, t = lax.axis_index("gr"), lax.axis_index("fs"), lax.axis_index("tp")
     z, y = f // inner, lax.rem(f, inner)
     rows, depth = normed.shape
@@ -104,11 +104,28 @@
         copy.start()
         sends.append(copy)
 
-    for o, i in [(o, 0) for o in range(1, outer)] + [(0, i) for i in range(1, inner)]:
-        n = o * inner + i
-        copy = rdma(normed, block_of(tok, n), tok_send.at[n], tok_recv.at[n], ahead(o, i))
+    for i in range(1, inner):
+        copy = rdma(normed, block_of(tok, i), tok_send.at[i], tok_recv.at[i], ahead(0, i))
         copy.start()
         sends.append(copy)
+
+    def beside(step):
+        return {"fs": (z + step) * inner + y}
+
+    def hop(o, step):
+        source = normed if o in (0, outer) else block_of(tok, o * inner)
+        n = (o + step) * inner
+        return rdma(source, block_of(tok, n), hop_send.at[o + step if step > 0 else outer + o + step], tok_recv.at[n], beside(step))
+
+    low, high = z > 0, z < outer - 1
+    hops = []
+
+    def move(o, step, when):
+        pl.when(when)(lambda: hop(o, step).start())
+        hops.append((o, step, when))
+
+    move(0, 1, high)
+    move(outer, -1, low)
 
     for sg in range(groups):
         def forward(sg=sg):
@@ -137,13 +154,21 @@
         pl.when(owner(sg) == t)(forward)
 
     for o in range(1, outer):
-        block = block_of(tok, o * inner)
-        rdma(block, block, tok_send.at[o * inner], tok_recv.at[o * inner], back(o, 0)).wait_recv()
-        for i in range(1, inner):
-            n = o * inner + i
-            copy = rdma(block, block_of(tok, n), tok_send.at[n], tok_recv.at[n], ahead(0, i))
-            copy.start()
-            sends.append(copy)
+        for n, when, step, more in ((o, z >= o, 1, high), (outer - o, z + o < outer, -1, low)):
+            block = block_of(tok, n * inner)
+
+            @pl.when(when)
+            def _(n=n, step=step, block=block):
+                rdma(block, block, tok_send.at[0], tok_recv.at[n * inner], beside(-step)).wait_recv()
+
+            if 0 < n + step < outer:
+                move(n, step, when & more)
+
+            @pl.when(when)
+            def _(n=n, block=block):
+                for i in range(1, inner):
+                    at = n * inner + i
+                    rdma(block, block_of(tok, at), tok_send.at[at], tok_recv.at[at], ahead(0, i)).start()
 
     for k, source in down_in:
         block = down_block(source, t)
@@ -200,7 +225,16 @@
         return rdma(block_of(part, n), block_of(got, n), part_send.at[n], part_recv.at[n], back(0, i))
 
     def far_copy(o):
-        return rdma(block_of(part, o * inner), block_of(far, o), far_send.at[o], far_recv.at[o], back(o, 0))
+        right = o > z
+        step = jnp.where(right, 1, -1)
+        last = jnp.where(right, o == outer - 1, o == 1)
+        slot = jnp.where(last, jnp.where(right, 0, outer), o + step)
+        return rdma(block_of(part, o * inner), block_of(far, slot), far_send.at[o], far_recv.at[slot],
+                    beside(step))
+
+    def far_arrived(slot, step):
+        rdma(block_of(far, slot), block_of(far, slot), far_send.at[0], far_recv.at[slot],
+             beside(step)).wait_recv()
 
     def compute(o):
         for i in range(1, inner):
@@ -235,44 +269,75 @@
     def add(o):
         gather(o)
 
+        def sum_up(passed):
+            def chunk(r, carry):
+                at = pl.multiple_of(r * 16, 16)
+                mine = pl.ds(pl.multiple_of(o * stack + at, 16), 16)
+                value = part[mine, :].astype(jnp.float32)
+                for i in range(1, inner):
+                    near = pl.ds(pl.multiple_of(o * stack + i * rows + at, 16), 16)
+                    value += got[near, :].astype(jnp.float32)
+                if passed:
+                    value += far[pl.ds(pl.multiple_of(o * rows + at, 16), 16), :].astype(jnp.float32)
+                part[mine, :] = value.astype(jnp.bfloat16)
+                return carry
+
+            lax.fori_loop(0, rows // 16, chunk, 0)
+
+        right = o > z
+        passed = (right & low) | (jnp.logical_not(right) & high)
+
+        @pl.when(passed)
+        def _():
+            far_arrived(o, jnp.where(right, -1, 1))
+            sum_up(True)
+
+        pl.when(jnp.logical_not(passed))(lambda: sum_up(False))
+        far_copy(o).start()
+
+    order = []
+    left_end, right_end = z * 0, z * 0 + outer - 1
+    for _ in range(outer):
+        take_left = z - left_end > right_end - z
+        owner_z = jnp.where(take_left, left_end, right_end)
+        order.append(lax.rem(z - owner_z + outer, outer))
+        left_end = jnp.where(take_left, left_end + 1, left_end)
+        right_end = jnp.where(take_left, right_end, right_end - 1)
+
+    for o in order:
+        compute(o)
+    for o in order[:-1]:
+        add(o)
+    gather(0)
+    pl.when(low)(lambda: far_arrived(0, -1))
+    pl.when(high)(lambda: far_arrived(outer, 1))
+
+    def total(ends):
         def chunk(r, carry):
             at = pl.multiple_of(r * 16, 16)
-            mine = pl.ds(pl.multiple_of(o * stack + at, 16), 16)
-            value = part[mine, :].astype(jnp.float32)
+            value = part[pl.ds(at, 16), :].astype(jnp.float32)
             for i in range(1, inner):
-                value += got[pl.ds(pl.multiple_of(o * stack + i * rows + at, 16), 16), :].astype(jnp.float32)
-            part[mine, :] = value.astype(jnp.bfloat16)
+                value += got[pl.ds(pl.multiple_of(i * rows + at, 16), 16), :].astype(jnp.float32)
+            for end in ends:
+                value += far[pl.ds(pl.multiple_of(end * rows + at, 16), 16), :].astype(jnp.float32)
+            served[pl.ds(at, 16), :] = value.astype(jnp.bfloat16)
             return carry
 
         lax.fori_loop(0, rows // 16, chunk, 0)
-        far_copy(o).start()
-
-    def step(o, carry):
-        compute(lax.rem(o, outer))
-        pl.when(o > 1)(lambda: add(o - 1))
-        return carry
-
-    lax.fori_loop(1, outer + 1, step, 0)
-    gather(0)
-
-    def finish(o, carry):
-        far_copy(o).wait()
-        return carry
-
-    lax.fori_loop(1, outer, finish, 0)
-
-    def total(r, carry):
-        at = pl.multiple_of(r * 16, 16)
-        value = part[pl.ds(at, 16), :].astype(jnp.float32)
-        for i in range(1, inner):
-            value += got[pl.ds(pl.multiple_of(i * rows + at, 16), 16), :].astype(jnp.float32)
-        for o in range(1, outer):
-            value += far[pl.ds(pl.multiple_of(o * rows + at, 16), 16), :].astype(jnp.float32)
-        served[pl.ds(at, 16), :] = value.astype(jnp.bfloat16)
-        return carry
-
-    lax.fori_loop(0, rows // 16, total, 0)
-
+
+    pl.when(low & high)(lambda: total((0, outer)))
+    pl.when(low & jnp.logical_not(high))(lambda: total((0,)))
+    pl.when(jnp.logical_not(low) & high)(lambda: total((outer,)))
+    pl.when(jnp.logical_not(low | high))(lambda: total(()))
+
+    for o, step, when in hops:
+        pl.when(when)(lambda o=o, step=step: hop(o, step).wait_send())
+    for n in range(inner, shards):
+        if n % inner:
+            block = block_of(tok, n)
+            rdma(block, block, tok_send.at[n], tok_recv.at[n], ahead(0, n % inner)).wait_send()
+    for o in range(1, outer):
+        far_copy(o).wait_send()
     for copy in sends:
         copy.wait_send()
 
@@ -328,7 +393,7 @@
             pltpu.VMEM((inner * rows, width), bf),
             pltpu.VMEM((shards * rows, depth), bf),
             pltpu.VMEM((shards * rows, depth), bf),
-            pltpu.VMEM((shards // inner * rows, depth), bf),
+            pltpu.VMEM(((shards // inner + 1) * rows, depth), bf),
             dma((nseg,)), dma((groups, shards)),
             dma((groups, groups, shards)), dma((groups, groups, shards)),
             dma((groups, groups, cores)), dma((groups, groups)),
@@ -336,7 +401,7 @@
             dma((cores, groups)), dma((cores, groups)),
             dma((shards,)), dma((shards,)),
             dma((shards,)), dma((shards,)),
-            dma((shards // inner,)), dma((shards // inner,)),
+            dma((shards // inner,)), dma((shards // inner + 1,)), dma((2 * (shards // inner),)),
             dma((2,)), dma((2,)),
         ],
         compiler_params=pltpu.CompilerParams(

time: 169 us -> 143 us (0.85)
  Pallas kernels: 156 us -> 129 us
    pallas_call x1, Pallas kernels: 156 us -> 129 us  [body(): pl.pallas_call(functools.partial(kernel, (groups, shards, cores)), out_sh...]
where the time goes in v3:
time: 143 us; the launch traced here: 142 us
  Pallas kernels  129 us (90%)
  local copies, waits for them, and re-layouts  7.63 us (5%)
  other arithmetic  4.54 us (3%)
    pallas_call x1, Pallas kernels, body(): pl.pallas_call(functools.partial(kernel, (groups, shards, cores)), out_sh...  129 us
    unnamed x7, local copies, waits for them, and re-layouts  7.63 us

profile of v3, /device:TPU:0, one launch (start us, length us, event | category | flops | bytes accessed | tf_op | source)
XLA Modules:
  0.0 142.2 jit_solution(8704341734538197843)
XLA Ops:
  0.6 1.2 fusion
  1.9 0.0 copy-start.1
  1.9 1.3 fusion.1.normed
  3.2 1.8 %multiply_convert_fusion.up = bf16[128,4096]{1,0:T(8,128)(2,1)S(1)} fusion(f32[128,4096]{1,0:T(8,128)} %param.6, f32[128]{0:T(128)} %param.5), kind=kLoop, calls=%fused_computation | loop fusion | flops 1048576 | bytes 3146240 | tf_op jit(solution)/shard_map/convert_element_type | solution.py:366
  5.0 0.0 copy-done.1
  5.1 0.2 convert_element_type.15.down
  5.2 129.4 %serve.1 = (bf16[128,2048]{1,0:T(8,128)(2,1)S(1)}, bf16[2048,1024]{1,0:T(8,128)(2,1)}, bf16[1024,2048]{1,0:T(8,128)(2,1)}) custom-call(bf16[128,2048]{1,0:T(8,128)(2,1)S(1)} %fusion.1.normed, bf16[128,4096]{1,0:T(8,128)(2,1)S(1)} %multiply_convert_fusion.up, bf16[512,1024]{1,0:T(8,128)(2,1)S(1)} %convert_element_type.15.down), custom_call_target="tpu_custom_call" | custom-call | tf_op jit(solution)/shard_map/serve/pallas_call | solution.py:380
  134.6 0.8 copy.10
  135.4 0.0 copy-start
  135.4 4.8 %copy.11 = bf16[2048,1024]{1,0:T(8,128)(2,1)} copy(bf16[2048,1024]{1,0:T(8,128)(2,1)} %get-tuple-element.7) | data formatting | bytes 8388608
  140.2 0.0 copy-done
  140.2 2.0 %copy.12 = bf16[1024,2048]{1,0:T(8,128)(2,1)} copy(bf16[1024,2048]{1,0:T(8,128)(2,1)S(1)} %copy-done) | data formatting | bytes 8388608
  (1 shorter events, 0.0 us)
Async XLA Ops:
  1.9 3.2 %copy-start.1 = (f32[512,1024]{1,0:T(8,128)S(1)}, f32[512,1024]{1,0:T(8,128)}, u32[]{:S(2)}) copy-start(f32[512,1024]{1,0:T(8,128)} %param.7) | copy-start | bytes 6291460
  135.4 4.8 %copy-start = (bf16[1024,2048]{1,0:T(8,128)(2,1)S(1)}, bf16[1024,2048]{1,0:T(8,128)(2,1)}, u32[]{:S(2)}) copy-start(bf16[1024,2048]{1,0:T(8,128)(2,1)} %get-tuple-element.8) | copy-start | bytes 12582916

commit v4 on v3

--- a/solution.py
+++ b/solution.py
@@ -20,7 +20,7 @@
     inner = inner_size(shards)
     outer = shards // inner
     (up_send, up_recv, gu_send, gu_recv, tu_send, tu_recv, gd_send, gd_recv,
-     td_send, td_recv, tok_send, tok_recv, part_send, part_recv, far_send, far_recv, hop_send, local, out_sem) = sems
+     td_send, td_recv, tok_send, tok_recv, part_send, part_recv, far_send, far_recv, hop_send, ou_send, ou_recv, local, out_sem) = sems
     g, f, t = lax.axis_index("gr"), lax.axis_index("fs"), lax.axis_index("tp")
     z, y = f // inner, lax.rem(f, inner)
     rows, depth = normed.shape
@@ -69,23 +69,6 @@
 
     def owner(sg):
         return (sg * shards + f) // nseg
-
-    def up_copy(i):
-        number = t * nseg + i
-        shard, sg = lax.rem(number, shards), number // shards
-        step = lax.rem(shard - f + shards, shards)
-        src = up.at[:, pl.ds(pl.multiple_of(i * segment, segment), segment)]
-        remote = rdma(src, up_block(g, f, sg), up_send.at[i], up_recv.at[sg, step], {"fs": shard})
-        here = pltpu.make_async_copy(src, up_block(g, f, sg), up_recv.at[sg, 0])
-        return shard == f, here, remote
-
-    def start_up(j, carry):
-        mine, here, remote = up_copy(lax.rem(f + j, nseg))
-        pl.when(mine)(here.start)
-        pl.when(jnp.logical_not(mine))(remote.start)
-        return carry
-
-    lax.fori_loop(0, nseg, start_up, 0)
 
     sends = []
     keep_down = pltpu.make_async_copy(down, down_block(g, t), local.at[0])
@@ -127,6 +110,43 @@
     move(0, 1, high)
     move(outer, -1, low)
 
+    def up_copy(i):
+        number = t * nseg + i
+        shard, sg = lax.rem(number, shards), number // shards
+        step = lax.rem(shard - f + shards, shards)
+        src = up.at[:, pl.ds(pl.multiple_of(i * segment, segment), segment)]
+        remote = rdma(src, up_block(g, f, sg), up_send.at[i], up_recv.at[sg, step], {"fs": shard})
+        here = pltpu.make_async_copy(src, up_block(g, f, sg), up_recv.at[sg, 0])
+        return shard == f, here, remote
+
+    def start_up(j, carry):
+        mine, here, remote = up_copy(lax.rem(f + j, nseg))
+        pl.when(mine)(here.start)
+        pl.when(jnp.logical_not(mine))(remote.start)
+        return carry
+
+    lax.fori_loop(0, nseg, start_up, 0)
+
+    def pass_on(o):
+        for n, when, step, more in ((o, z >= o, 1, high), (outer - o, z + o < outer, -1, low)):
+            block = block_of(tok, n * inner)
+
+            @pl.when(when)
+            def _(n=n, step=step, block=block):
+                rdma(block, block, tok_send.at[0], tok_recv.at[n * inner], beside(-step)).wait_recv()
+
+            if 0 < n + step < outer:
+                move(n, step, when & more)
+
+            @pl.when(when)
+            def _(n=n, block=block):
+                for i in range(1, inner):
+                    at = n * inner + i
+                    rdma(block, block_of(tok, at), tok_send.at[at], tok_recv.at[at], ahead(0, i)).start()
+
+    if outer > 1:
+        pass_on(1)
+
     for sg in range(groups):
         def forward(sg=sg):
             def arrived(k, carry):
@@ -153,22 +173,8 @@
 
         pl.when(owner(sg) == t)(forward)
 
-    for o in range(1, outer):
-        for n, when, step, more in ((o, z >= o, 1, high), (outer - o, z + o < outer, -1, low)):
-            block = block_of(tok, n * inner)
-
-            @pl.when(when)
-            def _(n=n, step=step, block=block):
-                rdma(block, block, tok_send.at[0], tok_recv.at[n * inner], beside(-step)).wait_recv()
-
-            if 0 < n + step < outer:
-                move(n, step, when & more)
-
-            @pl.when(when)
-            def _(n=n, block=block):
-                for i in range(1, inner):
-                    at = n * inner + i
-                    rdma(block, block_of(tok, at), tok_send.at[at], tok_recv.at[at], ahead(0, i)).start()
+    for o in range(2, outer):
+        pass_on(o)
 
     for k, source in down_in:
         block = down_block(source, t)
@@ -186,13 +192,12 @@
                 def arrived(k, carry):
                     block = up_block(source, lax.rem(f + shards - k, shards), sg)
                     rdma(block, block, gu_send.at[sg, d, k], gu_recv.at[sg, d, k], {"gr": source}).wait()
+                    for c in range(1, cores):
+                        rdma(block, block, ou_send.at[sg, d, c, k], ou_recv.at[sg, d, k],
+                             to("tp", t, cores, c)).start()
                     return carry
 
                 lax.fori_loop(0, shards, arrived, 0)
-                whole = up_group(source, sg)
-                for c in range(1, cores):
-                    rdma(whole, whole, tu_send.at[sg, d, c], tu_recv.at[sg, d],
-                         to("tp", t, cores, c)).start()
 
         pl.when(owner(sg) == t)(onward)
 
@@ -205,10 +210,16 @@
             rdma(block, block, td_send.at[c, k], td_recv.at[c, k], {"tp": core}).wait_recv()
     for sg in range(groups):
         def take(sg=sg):
-            for d in range(groups):
-                whole = up_group(lax.rem(g + groups - d, groups), sg)
-                rdma(whole, whole, tu_send.at[sg, d, 1], tu_recv.at[sg, d],
-                     {"tp": owner(sg)}).wait_recv()
+            whole = up_group(g, sg)
+            rdma(whole, whole, tu_send.at[sg, 0, 1], tu_recv.at[sg, 0], {"tp": owner(sg)}).wait_recv()
+            for d in range(1, groups):
+                def taken(k, carry):
+                    block = up_block(lax.rem(g + groups - d, groups), lax.rem(f + shards - k, shards), sg)
+                    rdma(block, block, tu_send.at[sg, 0, 1], ou_recv.at[sg, d, k],
+                         {"tp": owner(sg)}).wait_recv()
+                    return carry
+
+                lax.fori_loop(0, shards, taken, 0)
 
         pl.when(owner(sg) != t)(take)
 
@@ -349,11 +360,19 @@
     lax.fori_loop(0, nseg, end_up, 0)
     for sg in range(groups):
         def end(sg=sg):
-            for d in range(groups):
-                whole = up_group(lax.rem(g + groups - d, groups), sg)
-                for c in range(1, cores):
-                    rdma(whole, whole, tu_send.at[sg, d, c], tu_recv.at[sg, d],
-                         to("tp", t, cores, c)).wait_send()
+            whole = up_group(g, sg)
+            for c in range(1, cores):
+                rdma(whole, whole, tu_send.at[sg, 0, c], tu_recv.at[sg, 0],
+                     to("tp", t, cores, c)).wait_send()
+            for d in range(1, groups):
+                def left(k, carry):
+                    block = up_block(lax.rem(g + groups - d, groups), lax.rem(f + shards - k, shards), sg)
+                    for c in range(1, cores):
+                        rdma(block, block, ou_send.at[sg, d, c, k], ou_recv.at[sg, d, k],
+                             to("tp", t, cores, c)).wait_send()
+                    return carry
+
+                lax.fori_loop(0, shards, left, 0)
 
         pl.when(owner(sg) == t)(end)
     put_up.wait()
@@ -402,6 +421,7 @@
             dma((shards,)), dma((shards,)),
             dma((shards,)), dma((shards,)),
             dma((shards // inner,)), dma((shards // inner + 1,)), dma((2 * (shards // inner),)),
+            dma((groups, groups, cores, shards)), dma((groups, groups, shards)),
             dma((2,)), dma((2,)),
         ],
         compiler_params=pltpu.CompilerParams(

time: 143 us -> 142 us (level)
  no operation moved by 1% of the time
where the time goes in v4:
time: 142 us
  Pallas kernels  129 us (91%)
  local copies, waits for them, and re-layouts  7.63 us (5%)
  other arithmetic  4.54 us (3%)
    pallas_call x1, Pallas kernels, body(): pl.pallas_call(functools.partial(kernel, (groups, shards, cores)), out_sh...  129 us
    unnamed x7, local copies, waits for them, and re-layouts  7.63 us

profile of v4, /device:TPU:0, one launch (start us, length us, event | category | flops | bytes accessed | tf_op | source)
XLA Modules:
  0.0 141.9 jit_solution(10882690585171454112)
XLA Ops:
  0.6 1.2 fusion
  1.9 0.0 copy-start.1
  1.9 1.3 fusion.1.normed
  3.2 1.8 %multiply_convert_fusion.up = bf16[128,4096]{1,0:T(8,128)(2,1)S(1)} fusion(f32[128,4096]{1,0:T(8,128)} %param.6, f32[128]{0:T(128)} %param.5), kind=kLoop, calls=%fused_computation | loop fusion | flops 1048576 | bytes 3146240 | tf_op jit(solution)/shard_map/convert_element_type | solution.py:385
  5.0 0.0 copy-done.1
  5.1 0.2 convert_element_type.15.down
  5.2 129.0 %serve.1 = (bf16[128,2048]{1,0:T(8,128)(2,1)S(1)}, bf16[2048,1024]{1,0:T(8,128)(2,1)}, bf16[1024,2048]{1,0:T(8,128)(2,1)}) custom-call(bf16[128,2048]{1,0:T(8,128)(2,1)S(1)} %fusion.1.normed, bf16[128,4096]{1,0:T(8,128)(2,1)S(1)} %multiply_convert_fusion.up, bf16[512,1024]{1,0:T(8,128)(2,1)S(1)} %convert_element_type.15.down), custom_call_target="tpu_custom_call" | custom-call | tf_op jit(solution)/shard_map/serve/pallas_call | solution.py:399
  134.2 0.8 copy.10
  135.0 0.0 copy-start
  135.0 4.8 %copy.11 = bf16[2048,1024]{1,0:T(8,128)(2,1)} copy(bf16[2048,1024]{1,0:T(8,128)(2,1)} %get-tuple-element.7) | data formatting | bytes 8388608
  139.9 0.0 copy-done
  139.9 2.0 %copy.12 = bf16[1024,2048]{1,0:T(8,128)(2,1)} copy(bf16[1024,2048]{1,0:T(8,128)(2,1)S(1)} %copy-done) | data formatting | bytes 8388608
  (1 shorter events, 0.0 us)
Async XLA Ops:
  1.9 3.2 %copy-start.1 = (f32[512,1024]{1,0:T(8,128)S(1)}, f32[512,1024]{1,0:T(8,128)}, u32[]{:S(2)}) copy-start(f32[512,1024]{1,0:T(8,128)} %param.7) | copy-start | bytes 6291460
  135.0 4.8 %copy-start = (bf16[1024,2048]{1,0:T(8,128)(2,1)S(1)}, bf16[1024,2048]{1,0:T(8,128)(2,1)}, u32[]{:S(2)}) copy-start(bf16[1024,2048]{1,0:T(8,128)(2,1)} %get-tuple-element.8) | copy-start | bytes 12582916

commit v5 on v4

--- a/solution.py
+++ b/solution.py
@@ -15,12 +15,12 @@
     return max(d for d in range(1, shards + 1) if shards % d == 0 and d * d <= shards)
 
 
-def kernel(sizes, normed, up, down, served, out_up, out_down, tok, su, sd, hid, part, got, far, *sems):
+def kernel(sizes, normed, up, down, served, su, sd, tok, hid, part, got, far, *sems):
     groups, shards, cores = sizes
     inner = inner_size(shards)
     outer = shards // inner
     (up_send, up_recv, gu_send, gu_recv, tu_send, tu_recv, gd_send, gd_recv,
-     td_send, td_recv, tok_send, tok_recv, part_send, part_recv, far_send, far_recv, hop_send, ou_send, ou_recv, local, out_sem) = sems
+     td_send, td_recv, tok_send, tok_recv, part_send, part_recv, far_send, far_recv, hop_send, ou_send, ou_recv, local) = sems
     g, f, t = lax.axis_index("gr"), lax.axis_index("fs"), lax.axis_index("tp")
     z, y = f // inner, lax.rem(f, inner)
     rows, depth = normed.shape
@@ -223,11 +223,6 @@
 
         pl.when(owner(sg) != t)(take)
 
-    put_up = pltpu.make_async_copy(su, out_up, out_sem.at[0])
-    put_down = pltpu.make_async_copy(sd, out_down, out_sem.at[1])
-    put_up.start()
-    put_down.start()
-
     width = su.shape[1]
     stack = inner * rows
 
@@ -375,8 +370,6 @@
                 lax.fori_loop(0, shards, left, 0)
 
         pl.when(owner(sg) == t)(end)
-    put_up.wait()
-    put_down.wait()
 
 
 def body(tokens, norm_gain, up_weight, down_weight):
@@ -395,7 +388,6 @@
     bf = jnp.bfloat16
     dma = pltpu.SemaphoreType.DMA
     vmem = pl.BlockSpec(memory_space=pltpu.VMEM)
-    hbm = pl.BlockSpec(memory_space=pl.ANY)
     return pl.pallas_call(
         functools.partial(kernel, (groups, shards, cores)),
         out_shape=(
@@ -404,11 +396,9 @@
             jax.ShapeDtypeStruct((width, depth), bf),
         ),
         in_specs=[vmem] * 3,
-        out_specs=(vmem, hbm, hbm),
+        out_specs=(vmem, vmem, vmem),
         scratch_shapes=[
             pltpu.VMEM((shards * rows, depth), bf),
-            pltpu.VMEM((depth, width), bf),
-            pltpu.VMEM((width, depth), bf),
             pltpu.VMEM((inner * rows, width), bf),
             pltpu.VMEM((shards * rows, depth), bf),
             pltpu.VMEM((shards * rows, depth), bf),
@@ -422,10 +412,10 @@
             dma((shards,)), dma((shards,)),
             dma((shards // inner,)), dma((shards // inner + 1,)), dma((2 * (shards // inner),)),
             dma((groups, groups, cores, shards)), dma((groups, groups, shards)),
-            dma((2,)), dma((2,)),
+            dma((2,)),
         ],
         compiler_params=pltpu.CompilerParams(
-            collective_id=0, has_side_effects=True, vmem_limit_bytes=48 * 1024 * 1024
+            collective_id=0, has_side_effects=True, vmem_limit_bytes=34 * 1024 * 1024
         ),
         name="serve",
     )(normed, up, down)

time: 142 us -> 139 us (0.979)
  local copies, waits for them, and re-layouts: 7.63 us -> 4.82 us
    unnamed x7 -> x5, local copies, waits for them, and re-layouts: 7.63 us -> 4.82 us
where the time goes in v5:
time: 139 us
  Pallas kernels  129 us (93%)
  local copies, waits for them, and re-layouts  4.82 us (3%)
  other arithmetic  4.54 us (3%)
    pallas_call x1, Pallas kernels, body(): pl.pallas_call(functools.partial(kernel, (groups, shards, cores)), out_sh...  129 us
    unnamed x5, local copies, waits for them, and re-layouts  4.82 us

profile of v5, /device:TPU:0, one launch (start us, length us, event | category | flops | bytes accessed | tf_op | source)
XLA Modules:
  0.0 138.9 jit_solution(11535927334876288153)
XLA Ops:
  0.6 1.2 fusion
  1.9 0.0 copy-start
  1.9 1.3 fusion.1.normed
  3.2 1.8 %multiply_convert_fusion.up = bf16[128,4096]{1,0:T(8,128)(2,1)S(1)} fusion(f32[128,4096]{1,0:T(8,128)} %param.6, f32[128]{0:T(128)} %param.5), kind=kLoop, calls=%fused_computation | loop fusion | flops 1048576 | bytes 3146240 | tf_op jit(solution)/shard_map/convert_element_type | solution.py:378
  5.0 0.0 copy-done
  5.1 0.2 convert_element_type.15.down
  5.2 128.9 %serve.1 = (bf16[128,2048]{1,0:T(8,128)(2,1)S(1)}, bf16[2048,1024]{1,0:T(8,128)(2,1)S(1)}, bf16[1024,2048]{1,0:T(8,128)(2,1)S(1)}) custom-call(bf16[128,2048]{1,0:T(8,128)(2,1)S(1)} %fusion.1.normed, bf16[128,4096]{1,0:T(8,128)(2,1)S(1)} %multiply_convert_fusion.up, bf16[512,1024]{1,0:T(8,128)(2,1)S(1)} %convert_element_type.15.down), custom_call_target="tpu_custom_call" | custom-call | tf_op jit(solution)/shard_map/serve/pallas_call | solution.py:391
  134.1 0.8 copy.10
  134.9 2.0 %copy.11 = bf16[2048,1024]{1,0:T(8,128)(2,1)} copy(bf16[2048,1024]{1,0:T(8,128)(2,1)S(1)} %get-tuple-element.7) | data formatting | bytes 8388608
  136.9 2.0 %copy.12 = bf16[1024,2048]{1,0:T(8,128)(2,1)} copy(bf16[1024,2048]{1,0:T(8,128)(2,1)S(1)} %get-tuple-element.8) | data formatting | bytes 8388608
  (1 shorter events, 0.0 us)
Async XLA Ops:
  1.9 3.2 %copy-start = (f32[512,1024]{1,0:T(8,128)S(1)}, f32[512,1024]{1,0:T(8,128)}, u32[]{:S(2)}) copy-start(f32[512,1024]{1,0:T(8,128)} %param.7) | copy-start | bytes 6291460

commit v6 on v5

--- a/solution.py
+++ b/solution.py
@@ -8,7 +8,7 @@
 from jax.sharding import PartitionSpec as P
 
 MESH = pl.DeviceIdType.MESH
-TILE = 256
+TILE = 512
 
 
 def inner_size(shards):

time: 139 us -> 136 us (0.978)
  Pallas kernels: 129 us -> 126 us
    pallas_call x1, Pallas kernels: 129 us -> 126 us  [body(): pl.pallas_call(functools.partial(kernel, (groups, shards, cores)), out_sh...]
where the time goes in v6:
time: 136 us
  Pallas kernels  126 us (93%)
  local copies, waits for them, and re-layouts  4.82 us (4%)
  other arithmetic  4.54 us (3%)
    pallas_call x1, Pallas kernels, body(): pl.pallas_call(functools.partial(kernel, (groups, shards, cores)), out_sh...  126 us
    unnamed x5, local copies, waits for them, and re-layouts  4.82 us

profile of v6, /device:TPU:0, one launch (start us, length us, event | category | flops | bytes accessed | tf_op | source)
XLA Modules:
  0.0 136.1 jit_solution(2029954313726395260)
XLA Ops:
  0.6 1.2 fusion
  1.9 0.0 copy-start
  1.9 1.3 fusion.1.normed
  3.2 1.8 %multiply_convert_fusion.up = bf16[128,4096]{1,0:T(8,128)(2,1)S(1)} fusion(f32[128,4096]{1,0:T(8,128)} %param.6, f32[128]{0:T(128)} %param.5), kind=kLoop, calls=%fused_computation | loop fusion | flops 1048576 | bytes 3146240 | tf_op jit(solution)/shard_map/convert_element_type | solution.py:378
  5.0 0.0 copy-done
  5.1 0.2 convert_element_type.15.down
  5.2 126.0 %serve.1 = (bf16[128,2048]{1,0:T(8,128)(2,1)S(1)}, bf16[2048,1024]{1,0:T(8,128)(2,1)S(1)}, bf16[1024,2048]{1,0:T(8,128)(2,1)S(1)}) custom-call(bf16[128,2048]{1,0:T(8,128)(2,1)S(1)} %fusion.1.normed, bf16[128,4096]{1,0:T(8,128)(2,1)S(1)} %multiply_convert_fusion.up, bf16[512,1024]{1,0:T(8,128)(2,1)S(1)} %convert_element_type.15.down), custom_call_target="tpu_custom_call" | custom-call | tf_op jit(solution)/shard_map/serve/pallas_call | solution.py:391
  131.2 0.8 copy.10
  132.0 2.0 %copy.11 = bf16[2048,1024]{1,0:T(8,128)(2,1)} copy(bf16[2048,1024]{1,0:T(8,128)(2,1)S(1)} %get-tuple-element.7) | data formatting | bytes 8388608
  134.0 2.0 %copy.12 = bf16[1024,2048]{1,0:T(8,128)(2,1)} copy(bf16[1024,2048]{1,0:T(8,128)(2,1)S(1)} %get-tuple-element.8) | data formatting | bytes 8388608
  (1 shorter events, 0.0 us)
Async XLA Ops:
  1.9 3.2 %copy-start = (f32[512,1024]{1,0:T(8,128)S(1)}, f32[512,1024]{1,0:T(8,128)}, u32[]{:S(2)}) copy-start(f32[512,1024]{1,0:T(8,128)} %param.7) | copy-start | bytes 6291460
